TPU v7x, 32 devices: a whole 2x2x4 slice. The times are simulated.
32 devices in a mesh: sp: 8 (over z, x), tp: 4 (over y, core).
Axes of the slice: x: 2, y: 2, z: 4, core: 2. Of those that a mesh axis runs over, the one named last changes fastest.
Arguments:
- pool_input: bfloat16 [2048, 256], P('sp', 'tp'), may hold values from -6 to 6
- pool_weight: bfloat16 [4, 64, 64], P('tp'), may hold values from -0.75 to 0.75
- pool_gain: bfloat16 [256], P('tp'), may hold values from 0.099609375 to 1.8984375
- out_weight: bfloat16 [256, 2048], P(None, 'tp'), may hold values from -0.375 to 0.375
- resid: bfloat16 [2048, 2048], P('sp', 'tp'), may hold values from -90 to 90
- norm_gain: bfloat16 [2048], P('tp'), may hold values from 0.099609375 to 1.8984375
- routes: int32 [2048, 2], P('sp'), may hold values from 0 to 7, all different within a row; in each aligned block of 256 rows (0 to 255, 256 to 511, ...) at most 128 rows name the same one
- route_weight: float32 [2048, 2], P('sp'), may hold values from 0.2 to 1
- expert_gate: bfloat16 [8, 2048, 4096], P('sp', None, 'tp'), may hold values from -0.375 to 0.375
- expert_up: bfloat16 [8, 2048, 4096], P('sp', None, 'tp'), may hold values from -0.375 to 0.375
- expert_down: bfloat16 [8, 4096, 2048], P('sp', 'tp'), may hold values from -0.0234375 to 0.0234375
Outputs:
- layer_out: bfloat16 [2048, 2048], P('sp', 'tp')
Inputs may be any that keep to these rules, and one draw needn't show every extreme that they name: `routes`: the 2 experts of a position differ. In each aligned block of 256 positions no expert is named by more than 128 assignments; some block reaches that bound.
All inputs are finite; a program needn't handle non-finite values.
Results may differ from a plain program's by a relative error of at most 0.0085.
Values may be sent and summed in bfloat16 or wider, within the bound.
A program may use at most 64 MiB of HBM per device.

v0:
```python
import jax
import jax.numpy as jnp
from jax import lax
from jax.sharding import PartitionSpec as P

D = 2048
GSIZE = 64
REACH = 16
TOPK = 2
GATE_LIMIT = 7.0
GATE_ALPHA = 1.702
NORM_EPS = 1e-05


def from_behind(value, axis, steps):
    count = lax.axis_size(axis)
    first, last = (max(0, -steps), min(count, count - steps))
    return lax.ppermute(value, axis, [(source, source + steps) for source in range(first, last)])


def clamped_unit(gate_pre, up_pre):
    gate_cut = jnp.minimum(gate_pre, GATE_LIMIT)
    up_cut = jnp.clip(up_pre, -GATE_LIMIT, GATE_LIMIT)
    return (up_cut + 1.0) * gate_cut * jax.nn.sigmoid(GATE_ALPHA * gate_cut)


def window_pool(extended, width_of, position, tok_count):
    summed = jnp.zeros((tok_count, extended.shape[1]), jnp.float32)
    for offset in range(REACH):
        first_row = REACH - 1 - offset
        shifted = extended[first_row : first_row + tok_count]
        summed = summed + jnp.where(offset < width_of[None, :], shifted, 0.0)
    counted = jnp.minimum(position[:, None] + 1, width_of[None, :]).astype(jnp.float32)
    current = extended[REACH - 1 :]
    return (summed / counted - current).astype(jnp.bfloat16)


def slot_of(route_block, expert_count, capacity):
    flattened = route_block.reshape(-1)
    onehot = (flattened[:, None] == jnp.arange(expert_count, dtype=jnp.int32)[None, :]).astype(
        jnp.int32
    )
    earlier = jnp.cumsum(onehot, axis=0) - onehot
    ranked = jnp.sum(earlier * onehot, axis=1)
    return flattened * capacity + ranked


def on_device(
    pool_input,
    pool_weight,
    pool_gain,
    out_weight,
    resid,
    norm_gain,
    routes,
    route_weight,
    expert_gate,
    expert_up,
    expert_down,
):
    tok_rows, channels = pool_input.shape
    groups = pool_weight.shape[0]
    features = out_weight.shape[1]
    experts_all = lax.axis_size("sp") * expert_gate.shape[0]
    capacity = 2 * tok_rows * TOPK // experts_all
    tail_rows = pool_input[tok_rows - (REACH - 1) :]
    before = from_behind(tail_rows, "sp", 1)
    extended = jnp.concatenate([before, pool_input], axis=0).astype(jnp.float32)
    first_group = lax.axis_index("tp") * groups
    width_of = 2 ** (1 + (first_group + jnp.arange(channels, dtype=jnp.int32) // GSIZE) % 4)
    position = lax.axis_index("sp") * tok_rows + jnp.arange(tok_rows, dtype=jnp.int32)
    pooled = window_pool(extended, width_of, position, tok_rows)
    grouped = jnp.einsum(
        "tgc,gcd->tgd",
        pooled.reshape(tok_rows, groups, GSIZE),
        pool_weight,
        preferred_element_type=jnp.float32,
    )
    mixed_out = (
        (grouped * pool_gain.astype(jnp.float32).reshape(groups, GSIZE))
        .astype(jnp.bfloat16)
        .reshape(tok_rows, channels)
    )
    projected = jnp.dot(
        lax.all_gather(mixed_out, "tp", axis=1, tiled=True),
        out_weight,
        preferred_element_type=jnp.float32,
    )
    stored = lax.optimization_barrier((resid.astype(jnp.float32) + projected).astype(jnp.bfloat16))
    stream = stored.astype(jnp.float32)
    squares = lax.psum(jnp.sum(stream * stream, axis=1), "tp")
    scale_row = lax.rsqrt(squares / D + NORM_EPS)
    normed_part = (stream * scale_row[:, None] * norm_gain.astype(jnp.float32)).astype(jnp.bfloat16)
    slot_index = slot_of(routes, experts_all, capacity)
    token_ids = jnp.repeat(jnp.arange(tok_rows, dtype=jnp.int32), TOPK)
    slot_token = (
        jnp.full((experts_all * capacity,), tok_rows, jnp.int32).at[slot_index].set(token_ids)
    )
    sent_rows = jnp.take(normed_part, slot_token, axis=0, mode="fill", fill_value=0).reshape(
        experts_all, capacity, features
    )
    gathered = lax.all_gather(
        lax.all_to_all(sent_rows, "sp", split_axis=0, concat_axis=0, tiled=True),
        "tp",
        axis=2,
        tiled=True,
    )
    sources = gathered.shape[0]
    slot_count = gathered.shape[1]
    flattened = gathered.reshape(sources * slot_count, gathered.shape[2])
    gate_pre = jnp.dot(flattened, expert_gate[0], preferred_element_type=jnp.float32)
    up_pre = jnp.dot(flattened, expert_up[0], preferred_element_type=jnp.float32)
    hidden = clamped_unit(gate_pre, up_pre).astype(jnp.bfloat16)
    down_piece = expert_down[0]
    summed = lax.psum_scatter(
        lax.dot_general(
            down_piece, hidden, (((0,), (1,)), ((), ())), preferred_element_type=jnp.float32
        ).astype(jnp.bfloat16),
        "tp",
        scatter_dimension=0,
        tiled=True,
    ).astype(jnp.float32)
    result = summed.astype(jnp.bfloat16).reshape(summed.shape[0], sources, slot_count)
    returned = lax.all_to_all(result, "sp", split_axis=1, concat_axis=1, tiled=True)
    flat_back = returned.reshape(returned.shape[0], experts_all * capacity)
    picked = (
        jnp.take(flat_back, slot_index, axis=1)
        .astype(jnp.float32)
        .reshape(flat_back.shape[0], tok_rows, TOPK)
    )
    combined = jnp.sum(picked * route_weight[None, :, :], axis=2)
    return (stream + combined.T).astype(jnp.bfloat16)


def solution(mesh):
    in_specs = (
        P("sp", "tp"),
        P("tp", None, None),
        P("tp"),
        P(None, "tp"),
        P("sp", "tp"),
        P("tp"),
        P("sp", None),
        P("sp", None),
        P("sp", None, "tp"),
        P("sp", None, "tp"),
        P("sp", "tp", None),
    )
    out_specs = P("sp", "tp")
    return jax.shard_map(
        on_device, mesh=mesh, in_specs=in_specs, out_specs=out_specs, check_vma=False
    )
```

profile of v0, /device:TPU:0, one launch (start us, length us, event | category | flops | bytes accessed | tf_op | source)
XLA Modules:
  0.0 210.5 jit_solution(373483035602310403)
XLA Ops:
  6.5 0.0 copy-start
  6.5 0.0 all-gather.3.cloned.1.call-start
  6.5 0.8 slice.58
  7.4 4.9 %collective-permute-start = (bf16[15,64]{0,1:T(8,128)(2,1)S(1)}, bf16[15,64]{0,1:T(8,128)(2,1)S(1)}, u32[]{:S(2)}, u32[]{:S(2)}) collective-permute-start(bf16[15,64]{0,1:T(8,128)(2,1)S(1)} %slice.58), channel_id=1, source_target_pairs={{0,4},{4,8},{8,12},{12,16},{16,20},{20,24},{24,28},{1,5},{5,9},{9,... | collective-permute-start | bytes 5768 | tf_op jit(solution)/shard_map/ppermute | solution.py:18
  12.5 0.8 copy.18
  13.3 0.1 eq.28
  13.4 0.1 reshape.227
  13.6 0.7 broadcast_multiply_fusion
  14.3 1.1 reduce-window.6
  15.4 0.2 slice_reduce_fusion
  15.6 0.1 copy.22
  15.8 0.1 mul.320
  16.0 0.1 reshape.253
  16.1 0.1 fusion.39
  16.2 2.4 %scatter_custom_fusion = s32[1024]{0:T(1024)S(1)} fusion(s32[512]{0:T(512)S(1)} %bitcast.63, s32[512]{0:T(512)S(1)} %reshape.253, s32[]{:T(128)} %constant.149.clone.1), kind=kCustom, calls=%fused_computation.79 | custom fusion | bytes 4100 | tf_op jit(solution)/shard_map/scatter | solution.py:97
  18.7 0.7 convert_element_type.62
  19.4 0.7 convert_element_type.69
  20.1 0.0 collective-permute-done
  20.1 0.8 maximum_convert_fusion
  20.9 1.3 fusion.13
  22.2 5.4 %all-gather = bf16[256,1,256]{0,2,1:T(8,128)(2,1)S(1)} all-gather(bf16[256,1,64]{0,2,1:T(8,128)(2,1)S(1)} %fusion.13), channel_id=2, replica_groups=mesh['sp'=8,'tp'=4] {'tp'}, dimensions={2}, use_global_device_ids=true | all-gather | bytes 163840 | tf_op jit(solution)/shard_map/all_gather | solution.py:85
  27.7 0.0 copy-done
  27.7 1.2 fusion.10
  28.9 0.1 fusion.14
  29.0 7.1 %psum.7 = f32[256]{0:T(256)S(1)} all-reduce(f32[256]{0:T(256)S(1)} %fusion.14), channel_id=1, replica_groups=mesh['sp'=8,'tp'=4] {'tp'}, use_global_device_ids=true, to_apply=%region_5.6 | all-reduce | flops 256 | bytes 2048 | tf_op jit(solution)/shard_map/psum | solution.py:91
  36.1 0.1 fusion.16
  36.3 4.0 %gather_fusion = bf16[1024,512]{1,0:T(8,128)(2,1)S(1)} fusion(bf16[256,512]{1,0:T(8,128)(2,1)S(1)} %fusion.16, s32[1024]{0:T(1024)S(1)} %fusion.42), kind=kCustom, calls=%fused_computation | custom fusion | bytes 2101248 | tf_op jit(solution)/shard_map/jit(_take)/gather | solution.py:99
  40.2 0.2 broadcast_select_fusion
  40.5 29.1 %all_to_all.10 = bf16[8,128,512]{2,1,0:T(8,128)(2,1)} all-to-all(bf16[8,128,512]{2,1,0:T(8,128)(2,1)S(1)} %broadcast_select_fusion), channel_id=1, replica_groups=mesh['sp'=8,'tp'=4] {'sp'}, dimensions={0} | all-to-all | bytes 2097152 | tf_op jit(solution)/shard_map/all_to_all | solution.py:103
  69.6 0.0 all-gather.3.cloned.1.call-update
  69.6 0.0 reduce-scatter.2.cloned.1.call-start
  69.7 33.6 %all-gather.3.cloned.1.call-done = bf16[8,128,2048]{2,1,0:T(8,128)(2,1)} async-done(((bf16[8,128,512]{2,1,0:T(8,128)(2,1)}), bf16[8,128,2048]{2,1,0:T(8,128)(2,1)}) %all-gather.3.cloned.1.call-update) | async-done | bytes 4194320 | tf_op jit(solution)/shard_map/all_gather | solution.py:102
  103.3 0.0 copy-start.3
  103.3 0.0 copy-start.5
  103.3 7.6 %fusion.2 = f32[1024,1024]{1,0:T(8,128)S(1)} fusion(bf16[1024,2048]{1,0:T(8,128)(2,1)} %bitcast.65, bf16[1,2048,1024]{2,1,0:T(8,128)(2,1)} %param.19), kind=kOutput, calls=%fused_computation.5 | convolution fusion | flops 4294967296 | bytes 12582912 | tf_op jit(solution)/shard_map/dot_general | solution.py:111
  110.9 0.0 copy-done.3
  110.9 0.0 copy-done.5
  110.9 0.0 copy-start.4
  110.9 5.7 %multiply_convert_fusion = bf16[1024,1024]{1,0:T(8,128)(2,1)S(1)} fusion(f32[1024,1024]{1,0:T(8,128)S(1)} %fusion.2, bf16[1024,2048]{1,0:T(8,128)(2,1)S(1)} %bitcast.66, bf16[1,2048,1024]{2,1,0:T(8,128)(2,1)S(1)} %copy-done.3), kind=kOutput, calls=%fused_computation.10 | convolution fusion | flops 4305453056 | bytes 14680064 | tf_op jit(solution)/shard_map/dot_general | solution.py:112
  116.6 0.0 copy-done.4
  116.6 6.1 %convert_bitcast_fusion = bf16[2048,1024]{0,1:T(8,128)(2,1)} fusion(bf16[1024,1024]{1,0:T(8,128)(2,1)S(1)} %multiply_convert_fusion, bf16[1,1024,2048]{2,1,0:T(8,128)(2,1)S(1)} %copy-done.4), kind=kOutput, calls=%fused_computation.9 | convolution fusion | flops 4297064448 | bytes 10485760 | tf_op jit(solution)/shard_map/dot_general | solution.py:116
  122.7 0.0 copy-start.1
  122.7 0.0 copy-start.2
  122.7 0.0 reduce-scatter.2.cloned.1.call-update
  122.7 44.6 %reduce-scatter.2.cloned.1.call-done = bf16[512,1024]{0,1:T(8,128)(2,1)} async-done(((bf16[2048,1024]{0,1:T(8,128)(2,1)}), bf16[512,1024]{0,1:T(8,128)(2,1)}) %reduce-scatter.2.cloned.1.call-update) | async-done | bytes 1048592 | tf_op jit(solution)/shard_map/reduce_scatter | solution.py:115
  167.3 5.5 %all-to-all-start.1 = ((bf16[512,8,128]{0,2,1:T(8,128)(2,1)}), bf16[512,8,128]{0,2,1:T(8,128)(2,1)S(1)}, u32[]{:S(2)}, u32[]{:S(2)}) async-start(bf16[512,8,128]{0,2,1:T(8,128)(2,1)} %bitcast.61), calls=%async_computation.2 | async-start | bytes 2097152 | tf_op jit(solution)/shard_map/all_to_all | solution.py:124
  172.8 0.1 reduce_sum.32
  172.9 0.1 copy.20
  173.0 0.0 copy-done.1
  173.0 0.2 copy.21
  173.2 0.0 copy-done.2
  173.2 0.1 copy.23
  173.4 25.1 %all-to-all-done.1 = bf16[512,8,128]{0,2,1:T(8,128)(2,1)S(1)} async-done(((bf16[512,8,128]{0,2,1:T(8,128)(2,1)}), bf16[512,8,128]{0,2,1:T(8,128)(2,1)S(1)}, u32[]{:S(2)}, u32[]{:S(2)}) %all-to-all-start.1) | async-done | bytes 1048608 | tf_op jit(solution)/shard_map/all_to_all | solution.py:124
  198.5 2.0 gather_fusion.1
  200.4 0.2 gather.15
  200.6 2.2 %multiply_reduce_fusion = f32[512,256]{0,1:T(8,128)S(1)} fusion(bf16[512,256,2]{0,2,1:T(2,128)(2,1)S(1)} %gather.15, pred[256,2]{1,0:T(8,128)(4,1)S(1)} %copy.21, f32[256,2]{1,0:T(8,128)S(1)} %copy.23), kind=kLoop, calls=%fused_computation.17 | loop fusion | flops 917504 | bytes 1051136 | tf_op jit(solution)/shard_map/reduce_sum | solution.py:131
  202.9 0.8 fusion.17
  (20 shorter events, 0.3 us)
Async XLA Ops:
  6.5 21.1 %copy-start = (bf16[256,512]{1,0:T(8,128)(2,1)S(1)}, bf16[256,512]{1,0:T(8,128)(2,1)}, u32[]{:S(2)}) copy-start(bf16[256,512]{1,0:T(8,128)(2,1)} %param.14) | copy-start | bytes 786436
  6.5 96.7 %all-gather.3.cloned.1.call-start = ((), (), s32[]{:S(2)}) async-start(), calls=%async_computation.3 | async-start | bytes 5242880 | tf_op jit(solution)/shard_map/all_gather | solution.py:102
  7.4 12.7 %collective-permute-start = (bf16[15,64]{0,1:T(8,128)(2,1)S(1)}, bf16[15,64]{0,1:T(8,128)(2,1)S(1)}, u32[]{:S(2)}, u32[]{:S(2)}) collective-permute-start(bf16[15,64]{0,1:T(8,128)(2,1)S(1)} %slice.58), channel_id=1, source_target_pairs={{0,4},{4,8},{8,12},{12,16},{16,20},{20,24},{24,28},{1,5},{5,9},{9,... | collective-permute-start | bytes 5768 | tf_op jit(solution)/shard_map/ppermute | solution.py:18
  69.6 97.7 %reduce-scatter.2.cloned.1.call-start = ((), (), s32[]{:S(2)}) async-start(), calls=%async_computation.4 | async-start | bytes 5242880 | tf_op jit(solution)/shard_map/reduce_scatter | solution.py:115
  103.3 7.7 %copy-start.3 = (bf16[1,2048,1024]{2,1,0:T(8,128)(2,1)S(1)}, bf16[1,2048,1024]{2,1,0:T(8,128)(2,1)}, u32[]{:S(2)}) copy-start(bf16[1,2048,1024]{2,1,0:T(8,128)(2,1)} %param.20) | copy-start | bytes 12582916
  103.3 7.7 %copy-start.5 = (bf16[8,128,2048]{2,1,0:T(8,128)(2,1)S(1)}, bf16[8,128,2048]{2,1,0:T(8,128)(2,1)}, u32[]{:S(2)}) copy-start(bf16[8,128,2048]{2,1,0:T(8,128)(2,1)} %all-gather.3.cloned.1.call-done) | copy-start | bytes 12582916
  110.9 5.7 %copy-start.4 = (bf16[1,1024,2048]{2,1,0:T(8,128)(2,1)S(1)}, bf16[1,1024,2048]{2,1,0:T(8,128)(2,1)}, u32[]{:S(2)}) copy-start(bf16[1,1024,2048]{2,1,0:T(8,128)(2,1)} %param.21) | copy-start | bytes 12582916
  122.7 50.3 %copy-start.1 = (s32[256,2]{0,1:T(2,128)S(1)}, s32[256,2]{0,1:T(2,128)}, u32[]{:S(2)}) copy-start(s32[256,2]{0,1:T(2,128)} %param.17) | copy-start | bytes 6148
  122.7 50.5 %copy-start.2 = (f32[256,2]{0,1:T(2,128)S(1)}, f32[256,2]{0,1:T(2,128)}, u32[]{:S(2)}) copy-start(f32[256,2]{0,1:T(2,128)} %param.18) | copy-start | bytes 6148
  167.3 31.2 %all-to-all-start.1 = ((bf16[512,8,128]{0,2,1:T(8,128)(2,1)}), bf16[512,8,128]{0,2,1:T(8,128)(2,1)S(1)}, u32[]{:S(2)}, u32[]{:S(2)}) async-start(bf16[512,8,128]{0,2,1:T(8,128)(2,1)} %bitcast.61), calls=%async_computation.2 | async-start | bytes 2097152 | tf_op jit(solution)/shard_map/all_to_all | solution.py:124
Sparse Core Ops, SparseCore 0:
  69.7 33.4 all-gather.2
  122.8 44.3 reduce-scatter.1
where the time goes:
time: 211 us; the launch traced here: 210 us
  waiting for transfers between devices  103 us (49%)
  blocking collectives  41.7 us (20%)
  matrix products  21.9 us (10%)
  between operations  13.7 us (6%)
  local copies, waits for them, and re-layouts  11.7 us (6%)
  starting transfers between devices  10.4 us (5%)
  other arithmetic  7.86 us (4%)
    reduce_scatter x1, waiting for transfers between devices, on_device(): lax.psum_scatter(lax.dot_general(down_piece, hidden, (((0,), (1,)), ((),...  44.6 us
    all_gather x1, waiting for transfers between devices, on_device(): lax.all_gather(lax.all_to_all(sent_rows, 'sp', split_axis=0, concat_axis=...  33.6 us
    all_to_all x1, blocking collectives, on_device(): lax.all_to_all(sent_rows, 'sp', split_axis=0, concat_axis=0, tiled=True)  29.1 us
    all_to_all x1, waiting for transfers between devices, on_device(): lax.all_to_all(result, 'sp', split_axis=1, concat_axis=1, tiled=True)  25.1 us
    dot_general x1, matrix products, on_device(): jnp.dot(flattened, expert_gate[0], preferred_element_type=jnp.float32)  7.64 us
    psum x1, blocking collectives, on_device(): squares = lax.psum(jnp.sum(stream * stream, axis=1), 'tp')  7.13 us
    dot_general x1, matrix products, on_device(): lax.dot_general(down_piece, hidden, (((0,), (1,)), ((), ())), preferred_e...  6.07 us
    dot_general x1, matrix products, on_device(): jnp.dot(flattened, expert_up[0], preferred_element_type=jnp.float32)  5.66 us
  transfers between devices with their start and end apart: 4, of which 3 were waited for; matrix products, arithmetic and copies ran while one was open for 4% of the time, Pallas kernels for 0%

commit v1 on v0

--- a/solution.py
+++ b/solution.py
@@ -121,7 +121,10 @@
         tiled=True,
     ).astype(jnp.float32)
     result = summed.astype(jnp.bfloat16).reshape(summed.shape[0], sources, slot_count)
-    returned = lax.all_to_all(result, "sp", split_axis=1, concat_axis=1, tiled=True)
+    returned = jnp.concatenate(
+        lax.all_to_all(jnp.stack(jnp.split(result, lax.axis_size("sp"), axis=1)), "sp", 0, 0),
+        axis=1,
+    )
     flat_back = returned.reshape(returned.shape[0], experts_all * capacity)
     picked = (
         jnp.take(flat_back, slot_index, axis=1)

time: 211 us -> 224 us (1.062)
  local copies, waits for them, and re-layouts: 11.7 us -> 24.2 us
    unnamed x14 -> x21, local copies, waits for them, and re-layouts: 0.97 us -> 11.9 us
where the time goes in v1:
time: 224 us; the launch traced here: 223 us
  waiting for transfers between devices  103 us (46%)
  blocking collectives  41.7 us (19%)
  local copies, waits for them, and re-layouts  24.2 us (11%)
  matrix products  21.9 us (10%)
  between operations  13.7 us (6%)
  starting transfers between devices  10.4 us (5%)
  other arithmetic  7.86 us (4%)
    reduce_scatter x1, waiting for transfers between devices, on_device(): lax.psum_scatter(lax.dot_general(down_piece, hidden, (((0,), (1,)), ((),...  44.6 us
    all_gather x1, waiting for transfers between devices, on_device(): lax.all_gather(lax.all_to_all(sent_rows, 'sp', split_axis=0, concat_axis=...  33.6 us
    all_to_all x1, blocking collectives, on_device(): lax.all_to_all(sent_rows, 'sp', split_axis=0, concat_axis=0, tiled=True)  29.1 us
    all_to_all x1, waiting for transfers between devices, on_device(): lax.all_to_all(jnp.stack(jnp.split(result, lax.axis_size('sp'), axis=1)),...  25.1 us
    unnamed x21, local copies, waits for them, and re-layouts  11.9 us
    dot_general x1, matrix products, on_device(): jnp.dot(flattened, expert_gate[0], preferred_element_type=jnp.float32)  7.64 us
    psum x1, blocking collectives, on_device(): squares = lax.psum(jnp.sum(stream * stream, axis=1), 'tp')  7.13 us
    dot_general x1, matrix products, on_device(): lax.dot_general(down_piece, hidden, (((0,), (1,)), ((), ())), preferred_e...  6.07 us
  transfers between devices with their start and end apart: 4, of which 3 were waited for; matrix products, arithmetic and copies ran while one was open for 4% of the time, Pallas kernels for 0%

profile of v1, /device:TPU:0, one launch (start us, length us, event | category | flops | bytes accessed | tf_op | source)
XLA Modules:
  0.0 223.0 jit_solution(5382660900606504322)
XLA Ops:
  6.5 0.0 copy-start
  6.5 0.0 all-gather.3.cloned.1.call-start
  6.5 0.8 slice.58
  7.4 4.9 %collective-permute-start = (bf16[15,64]{0,1:T(8,128)(2,1)S(1)}, bf16[15,64]{0,1:T(8,128)(2,1)S(1)}, u32[]{:S(2)}, u32[]{:S(2)}) collective-permute-start(bf16[15,64]{0,1:T(8,128)(2,1)S(1)} %slice.58), channel_id=1, source_target_pairs={{0,4},{4,8},{8,12},{12,16},{16,20},{20,24},{24,28},{1,5},{5,9},{9,... | collective-permute-start | bytes 5768 | tf_op jit(solution)/shard_map/ppermute | solution.py:18
  12.5 0.8 copy.18
  13.3 0.1 eq.28
  13.4 0.1 reshape.227
  13.6 0.7 broadcast_multiply_fusion
  14.3 1.1 reduce-window.6
  15.4 0.2 slice_reduce_fusion
  15.6 0.1 copy.22
  15.8 0.1 mul.320
  16.0 0.1 reshape.253
  16.1 0.1 fusion.47
  16.2 2.4 %scatter_custom_fusion = s32[1024]{0:T(1024)S(1)} fusion(s32[512]{0:T(512)S(1)} %bitcast.104, s32[512]{0:T(512)S(1)} %reshape.253, s32[]{:T(128)} %constant.149.clone.1), kind=kCustom, calls=%fused_computation.95 | custom fusion | bytes 4100 | tf_op jit(solution)/shard_map/scatter | solution.py:97
  18.7 0.7 convert_element_type.62
  19.4 0.7 convert_element_type.69
  20.1 0.0 collective-permute-done
  20.1 0.8 maximum_convert_fusion
  20.9 1.3 fusion.13
  22.2 5.4 %all-gather = bf16[256,1,256]{0,2,1:T(8,128)(2,1)S(1)} all-gather(bf16[256,1,64]{0,2,1:T(8,128)(2,1)S(1)} %fusion.13), channel_id=2, replica_groups=mesh['sp'=8,'tp'=4] {'tp'}, dimensions={2}, use_global_device_ids=true | all-gather | bytes 163840 | tf_op jit(solution)/shard_map/all_gather | solution.py:85
  27.7 0.0 copy-done
  27.7 1.2 fusion.10
  28.9 0.1 fusion.14
  29.0 7.1 %psum.7 = f32[256]{0:T(256)S(1)} all-reduce(f32[256]{0:T(256)S(1)} %fusion.14), channel_id=1, replica_groups=mesh['sp'=8,'tp'=4] {'tp'}, use_global_device_ids=true, to_apply=%region_5.6 | all-reduce | flops 256 | bytes 2048 | tf_op jit(solution)/shard_map/psum | solution.py:91
  36.1 0.1 fusion.16
  36.3 4.0 %gather_fusion = bf16[1024,512]{1,0:T(8,128)(2,1)S(1)} fusion(bf16[256,512]{1,0:T(8,128)(2,1)S(1)} %fusion.16, s32[1024]{0:T(1024)S(1)} %fusion.50), kind=kCustom, calls=%fused_computation | custom fusion | bytes 2101248 | tf_op jit(solution)/shard_map/jit(_take)/gather | solution.py:99
  40.2 0.2 broadcast_select_fusion
  40.5 29.1 %all_to_all.10 = bf16[8,128,512]{2,1,0:T(8,128)(2,1)} all-to-all(bf16[8,128,512]{2,1,0:T(8,128)(2,1)S(1)} %broadcast_select_fusion), channel_id=1, replica_groups=mesh['sp'=8,'tp'=4] {'sp'}, dimensions={0} | all-to-all | bytes 2097152 | tf_op jit(solution)/shard_map/all_to_all | solution.py:103
  69.6 0.0 all-gather.3.cloned.1.call-update
  69.6 0.0 reduce-scatter.2.cloned.1.call-start
  69.7 33.6 %all-gather.3.cloned.1.call-done = bf16[8,128,2048]{2,1,0:T(8,128)(2,1)} async-done(((bf16[8,128,512]{2,1,0:T(8,128)(2,1)}), bf16[8,128,2048]{2,1,0:T(8,128)(2,1)}) %all-gather.3.cloned.1.call-update) | async-done | bytes 4194320 | tf_op jit(solution)/shard_map/all_gather | solution.py:102
  103.3 0.0 copy-start.3
  103.3 0.0 copy-start.5
  103.3 7.6 %fusion.2 = f32[1024,1024]{1,0:T(8,128)S(1)} fusion(bf16[1024,2048]{1,0:T(8,128)(2,1)} %bitcast.106, bf16[1,2048,1024]{2,1,0:T(8,128)(2,1)} %param.19), kind=kOutput, calls=%fused_computation.5 | convolution fusion | flops 4294967296 | bytes 12582912 | tf_op jit(solution)/shard_map/dot_general | solution.py:111
  110.9 0.0 copy-done.3
  110.9 0.0 copy-done.5
  110.9 0.0 copy-start.4
  110.9 5.7 %multiply_convert_fusion = bf16[1024,1024]{1,0:T(8,128)(2,1)S(1)} fusion(f32[1024,1024]{1,0:T(8,128)S(1)} %fusion.2, bf16[1024,2048]{1,0:T(8,128)(2,1)S(1)} %bitcast.107, bf16[1,2048,1024]{2,1,0:T(8,128)(2,1)S(1)} %copy-done.3), kind=kOutput, calls=%fused_computation.10 | convolution fusion | flops 4305453056 | bytes 14680064 | tf_op jit(solution)/shard_map/dot_general | solution.py:112
  116.6 0.0 copy-done.4
  116.6 6.1 %convert_bitcast_fusion = bf16[2048,1024]{0,1:T(8,128)(2,1)} fusion(bf16[1024,1024]{1,0:T(8,128)(2,1)S(1)} %multiply_convert_fusion, bf16[1,1024,2048]{2,1,0:T(8,128)(2,1)S(1)} %copy-done.4), kind=kOutput, calls=%fused_computation.9 | convolution fusion | flops 4297064448 | bytes 10485760 | tf_op jit(solution)/shard_map/dot_general | solution.py:116
  122.7 0.0 copy-start.1
  122.7 0.0 reduce-scatter.2.cloned.1.call-update
  122.7 44.6 %reduce-scatter.2.cloned.1.call-done = bf16[512,1024]{0,1:T(8,128)(2,1)} async-done(((bf16[2048,1024]{0,1:T(8,128)(2,1)}), bf16[512,1024]{0,1:T(8,128)(2,1)}) %reduce-scatter.2.cloned.1.call-update) | async-done | bytes 1048592 | tf_op jit(solution)/shard_map/reduce_scatter | solution.py:115
  167.3 1.5 fusion.25
  168.8 1.6 fusion.24
  170.4 1.6 fusion.23
  172.0 1.6 fusion.22
  173.5 1.6 fusion.21
  175.1 1.5 fusion.20
  176.6 1.6 fusion.19
  178.2 1.6 fusion.18
  179.8 5.5 %all-to-all-start.1 = ((bf16[8,512,1,128]{1,3,2,0:T(8,128)(2,1)}), bf16[8,512,1,128]{1,3,2,0:T(8,128)(2,1)S(1)}, u32[]{:S(2)}, u32[]{:S(2)}) async-start(bf16[8,512,1,128]{1,3,2,0:T(8,128)(2,1)} %fusion.18), calls=%async_computation.2 | async-start | bytes 2097152 | tf_op jit(solution)/shard_map/all_to_all | solution.py:125
  185.3 0.1 reduce_sum.32
  185.4 0.1 copy.20
  185.5 0.0 copy-done.1
  185.5 0.2 copy.21
  185.7 0.0 copy-done.2
  185.7 0.1 copy.23
  185.9 25.1 %all-to-all-done.1 = bf16[8,512,1,128]{1,3,2,0:T(8,128)(2,1)S(1)} async-done(((bf16[8,512,1,128]{1,3,2,0:T(8,128)(2,1)}), bf16[8,512,1,128]{1,3,2,0:T(8,128)(2,1)S(1)}, u32[]{:S(2)}, u32[]{:S(2)}) %all-to-all-start.1) | async-done | bytes 1048608 | tf_op jit(solution)/shard_map/all_to_all | solution.py:125
  211.0 2.0 gather_fusion.1
  212.9 0.2 gather.15
  213.1 2.2 multiply_reduce_fusion
  215.4 0.8 fusion.17
  (21 shorter events, 0.3 us)
Async XLA Ops:
  6.5 21.1 %copy-start = (bf16[256,512]{1,0:T(8,128)(2,1)S(1)}, bf16[256,512]{1,0:T(8,128)(2,1)}, u32[]{:S(2)}) copy-start(bf16[256,512]{1,0:T(8,128)(2,1)} %param.14) | copy-start | bytes 786436
  6.5 96.7 %all-gather.3.cloned.1.call-start = ((), (), s32[]{:S(2)}) async-start(), calls=%async_computation.3 | async-start | bytes 5242880 | tf_op jit(solution)/shard_map/all_gather | solution.py:102
  7.4 12.7 %collective-permute-start = (bf16[15,64]{0,1:T(8,128)(2,1)S(1)}, bf16[15,64]{0,1:T(8,128)(2,1)S(1)}, u32[]{:S(2)}, u32[]{:S(2)}) collective-permute-start(bf16[15,64]{0,1:T(8,128)(2,1)S(1)} %slice.58), channel_id=1, source_target_pairs={{0,4},{4,8},{8,12},{12,16},{16,20},{20,24},{24,28},{1,5},{5,9},{9,... | collective-permute-start | bytes 5768 | tf_op jit(solution)/shard_map/ppermute | solution.py:18
  69.6 97.7 %reduce-scatter.2.cloned.1.call-start = ((), (), s32[]{:S(2)}) async-start(), calls=%async_computation.4 | async-start | bytes 5242880 | tf_op jit(solution)/shard_map/reduce_scatter | solution.py:115
  103.3 7.7 %copy-start.3 = (bf16[1,2048,1024]{2,1,0:T(8,128)(2,1)S(1)}, bf16[1,2048,1024]{2,1,0:T(8,128)(2,1)}, u32[]{:S(2)}) copy-start(bf16[1,2048,1024]{2,1,0:T(8,128)(2,1)} %param.20) | copy-start | bytes 12582916
  103.3 7.7 %copy-start.5 = (bf16[8,128,2048]{2,1,0:T(8,128)(2,1)S(1)}, bf16[8,128,2048]{2,1,0:T(8,128)(2,1)}, u32[]{:S(2)}) copy-start(bf16[8,128,2048]{2,1,0:T(8,128)(2,1)} %all-gather.3.cloned.1.call-done) | copy-start | bytes 12582916
  110.9 5.7 %copy-start.4 = (bf16[1,1024,2048]{2,1,0:T(8,128)(2,1)S(1)}, bf16[1,1024,2048]{2,1,0:T(8,128)(2,1)}, u32[]{:S(2)}) copy-start(bf16[1,1024,2048]{2,1,0:T(8,128)(2,1)} %param.21) | copy-start | bytes 12582916
  122.7 62.8 %copy-start.1 = (s32[256,2]{0,1:T(2,128)S(1)}, s32[256,2]{0,1:T(2,128)}, u32[]{:S(2)}) copy-start(s32[256,2]{0,1:T(2,128)} %param.17) | copy-start | bytes 6148
  122.7 63.0 %copy-start.2 = (f32[256,2]{0,1:T(2,128)S(1)}, f32[256,2]{0,1:T(2,128)}, u32[]{:S(2)}) copy-start(f32[256,2]{0,1:T(2,128)} %param.18) | copy-start | bytes 6148
  179.8 31.2 %all-to-all-start.1 = ((bf16[8,512,1,128]{1,3,2,0:T(8,128)(2,1)}), bf16[8,512,1,128]{1,3,2,0:T(8,128)(2,1)S(1)}, u32[]{:S(2)}, u32[]{:S(2)}) async-start(bf16[8,512,1,128]{1,3,2,0:T(8,128)(2,1)} %fusion.18), calls=%async_computation.2 | async-start | bytes 2097152 | tf_op jit(solution)/shard_map/all_to_all | solution.py:125
Sparse Core Ops, SparseCore 0:
  69.7 33.4 all-gather.2
  122.8 44.3 reduce-scatter.1
